TPU v7x, 32 devices: a whole 2x2x4 slice. The times are simulated.
32 devices in a mesh: ep: 16 (over z, y, x), tp: 2 (over core).
Axes of the slice: x: 2, y: 2, z: 4, core: 2. Of those that a mesh axis runs over, the one named last changes fastest.
Arguments:
- residual: bfloat16 [1024, 2048], P('ep', 'tp'), may hold values from -100 to 100
- route_ids: int32 [1024, 4], P('ep'), may hold values from 0 to 15, all different within a row; in each aligned block of 64 rows (0 to 63, 64 to 127, ...) at most 24 rows name the same one
- route_weights: float32 [1024, 4], P('ep'), may hold values from 0.1 to 1
- carried_state: float32 [2, 1024, 4096], P(None, 'ep', 'tp'), may hold values from -6 to 6
- mix_gain: float32 [2048], replicated, may hold values from 0.1 to 1.9
- in_proj: bfloat16 [2048, 1024], P(None, 'tp'), may hold values from -0.125 to 0.125
- decay_rate: float32 [64, 64], P('tp'), may hold values from 0.1 to 2
- frequency: float32 [64, 64], P('tp'), may hold values from -3 to 3
- step_size: float32 [64], P('tp'), may hold values from 0.05 to 1
- input_map: float32 [2, 64, 64, 16], P(None, 'tp'), may hold values from -1.5 to 1.5
- output_matrix: float32 [2, 64, 16, 64], P(None, 'tp'), may hold values from -0.5 to 0.5
- passthrough_scale: float32 [1024], P('tp'), may hold values from -4 to 4
- out_gain: float32 [1024], replicated, may hold values from 0.1 to 1.9
- out_proj: bfloat16 [1024, 2048], P(None, 'tp'), may hold values from -0.1875 to 0.1875
- ffn_gain: float32 [2048], replicated, may hold values from 0.1 to 1.9
- w_gate: bfloat16 [16, 2048, 2048], P('ep', None, 'tp'), may hold values from -5 to 5
- w_up: bfloat16 [16, 2048, 2048], P('ep', None, 'tp'), may hold values from -5 to 5
- w_down: bfloat16 [16, 2048, 2048], P('ep', 'tp'), may hold values from -0.125 to 0.125
Outputs:
- updated: bfloat16 [1024, 2048], P('ep', 'tp')
- new_state: float32 [2, 1024, 4096], P(None, 'ep', 'tp')
Inputs may be any that keep to these rules, and one draw needn't show every extreme that they name: `route_ids`: each row names 4 different experts. Among the 64 rows of one device (aligned blocks) no expert is named more than 24 times, and in every draw some block names some expert exactly 24 times.
All inputs are finite; a program needn't handle non-finite values.
Results may differ from a plain program's by a relative error of at most 0.018.
Values may be sent and summed in bfloat16 or wider, within the bound.
No kernel may reach another device: no remote copies, remote signals or barrier semaphores. Data moves between devices by JAX's collectives and lax.ppermute only.
A program may use at most 128 MiB of HBM per device.

v0:
```python
import jax
import jax.numpy as jnp
from jax import lax
from jax.sharding import PartitionSpec as P

epsilon = 1e-06
clamp_limit = 7.0
swish_alpha = 1.702


def rms_rows(values, gain_vec):
    return values * lax.rsqrt(jnp.mean(values * values, axis=1, keepdims=True) + epsilon) * gain_vec


def discretize(decay_rate, frequency, step_size):
    rate_real = -decay_rate
    time_step = step_size[:, None]
    magnitude = jnp.exp(rate_real * time_step)
    phase_angle = frequency * time_step
    bar_real = magnitude * jnp.cos(phase_angle)
    bar_imag = magnitude * jnp.sin(phase_angle)
    denominator = rate_real * rate_real + frequency * frequency
    shifted = bar_real - 1.0
    coef_real = (shifted * rate_real + bar_imag * frequency) / denominator
    coef_imag = (bar_imag * rate_real - shifted * frequency) / denominator
    return (bar_real, bar_imag, coef_real, coef_imag)


def state_step(
    channels,
    carried_state,
    decay_rate,
    frequency,
    step_size,
    input_map,
    output_matrix,
    passthrough_scale,
):
    row_count = channels.shape[0]
    number_of_groups, state_width = decay_rate.shape
    channels_per_group = input_map.shape[3]
    bar_real, bar_imag, coef_real, coef_imag = discretize(decay_rate, frequency, step_size)
    map_real = coef_real[..., None] * input_map[0] - coef_imag[..., None] * input_map[1]
    map_imag = coef_real[..., None] * input_map[1] + coef_imag[..., None] * input_map[0]
    input_rows = channels.astype(jnp.float32).reshape(
        row_count, number_of_groups, channels_per_group
    )
    largest_precision = lax.Precision.HIGHEST
    push_real = jnp.einsum("sgc,gpc->sgp", input_rows, map_real, precision=largest_precision)
    push_imag = jnp.einsum("sgc,gpc->sgp", input_rows, map_imag, precision=largest_precision)
    old_real = carried_state[0].reshape(row_count, number_of_groups, state_width)
    old_imag = carried_state[1].reshape(row_count, number_of_groups, state_width)
    updated_real = bar_real * old_real - bar_imag * old_imag + push_real
    updated_imaginary = bar_real * old_imag + bar_imag * old_real + push_imag
    mixer_output = (
        jnp.einsum("dfk,idk->idf", output_matrix[0], updated_real, precision=largest_precision)
        - jnp.einsum(
            "dfk,idk->idf", output_matrix[1], updated_imaginary, precision=largest_precision
        )
        + passthrough_scale.reshape(number_of_groups, channels_per_group) * input_rows
    )
    activated = jax.nn.gelu(
        mixer_output.reshape(row_count, number_of_groups * channels_per_group)
    ).astype(jnp.bfloat16)
    new_state = jnp.stack(
        [updated_real.reshape(row_count, -1), updated_imaginary.reshape(row_count, -1)]
    )
    return (activated, new_state)


def own_slice(vector, width):
    return lax.dynamic_slice_in_dim(vector, lax.axis_index("tp") * width, width)


def local(
    residual,
    route_ids,
    route_weights,
    carried_state,
    mix_gain,
    in_proj,
    decay_rate,
    frequency,
    step_size,
    input_map,
    output_matrix,
    passthrough_scale,
    out_gain,
    out_proj,
    ffn_gain,
    w_gate,
    w_up,
    w_down,
):
    row_count, half_width = residual.shape
    top_count = route_ids.shape[1]
    local_experts = w_gate.shape[0]
    peer_count = lax.axis_size("ep")
    expert_count = local_experts * peer_count
    capacity = max(2, 3 * row_count * top_count // (2 * expert_count))
    whole_rows = lax.all_gather(residual, "tp", axis=1, tiled=True)
    normed_rows = rms_rows(whole_rows.astype(jnp.float32), mix_gain).astype(jnp.bfloat16)
    channels = jnp.dot(normed_rows, in_proj, preferred_element_type=jnp.float32).astype(
        jnp.bfloat16
    )
    activated, new_state = state_step(
        channels,
        carried_state,
        decay_rate,
        frequency,
        step_size,
        input_map,
        output_matrix,
        passthrough_scale,
    )
    channel_width = activated.shape[1]
    own_half = activated.astype(jnp.float32)
    total_sq = lax.psum(jnp.sum(own_half * own_half, axis=1), "tp")
    full_width = channel_width * lax.axis_size("tp")
    row_scale = lax.rsqrt(total_sq / full_width + epsilon)[:, None]
    local_scaled = (own_half * row_scale * own_slice(out_gain, channel_width)).astype(jnp.bfloat16)
    scaled = lax.all_gather(local_scaled, "tp", axis=1, tiled=True)
    after_mixer = (
        residual.astype(jnp.float32) + jnp.dot(scaled, out_proj, preferred_element_type=jnp.float32)
    ).astype(jnp.bfloat16)
    flat_ids = route_ids.reshape(row_count * top_count)
    onehot = (flat_ids[:, None] == jnp.arange(expert_count, dtype=jnp.int32)[None, :]).astype(
        jnp.int32
    )
    before = jnp.cumsum(onehot, axis=0) - onehot
    slot_index = jnp.sum(before * onehot, axis=1)
    position = flat_ids * capacity + slot_index
    slot_table = jnp.any(
        jnp.arange(expert_count * capacity, dtype=jnp.int32)[:, None, None]
        == position.reshape(row_count, top_count)[None, :, :],
        axis=2,
    ).astype(jnp.bfloat16)
    own_half = after_mixer.astype(jnp.float32)
    total_sq = lax.psum(jnp.sum(own_half * own_half, axis=1), "tp")
    full_width = half_width * lax.axis_size("tp")
    row_scale = lax.rsqrt(total_sq / full_width + epsilon)[:, None]
    expert_in = (own_half * row_scale * own_slice(ffn_gain, half_width)).astype(jnp.bfloat16)
    buffer = jnp.dot(slot_table, expert_in, preferred_element_type=jnp.float32).astype(jnp.bfloat16)
    buffer = buffer.reshape(peer_count, local_experts, capacity, half_width)
    arrived = lax.all_gather(
        lax.all_to_all(buffer, "ep", split_axis=0, concat_axis=0, tiled=True),
        "tp",
        axis=3,
        tiled=True,
    )
    gate_pre = jnp.einsum("necd,edf->necf", arrived, w_gate, preferred_element_type=jnp.float32)
    up_pre = jnp.einsum("necd,edf->necf", arrived, w_up, preferred_element_type=jnp.float32)
    gated = jnp.minimum(gate_pre, clamp_limit)
    activation = (
        (jnp.clip(up_pre, -clamp_limit, clamp_limit) + 1.0)
        * gated
        * jax.nn.sigmoid(swish_alpha * gated)
    ).astype(jnp.bfloat16)
    partial_value = jnp.einsum(
        "necf,efd->necd", activation, w_down, preferred_element_type=jnp.float32
    )
    partial_value = lax.optimization_barrier(partial_value.astype(jnp.bfloat16)).astype(jnp.float32)
    summed = lax.psum_scatter(
        partial_value.astype(jnp.bfloat16), "tp", scatter_dimension=3, tiled=True
    )
    result = lax.all_to_all(summed, "ep", split_axis=0, concat_axis=0, tiled=True)
    returned = result.reshape(expert_count * capacity, half_width)
    picked = returned[position].reshape(row_count, top_count, half_width)
    expert_sum = jnp.sum(route_weights[:, :, None] * picked.astype(jnp.float32), axis=1)
    updated = (after_mixer.astype(jnp.float32) + expert_sum).astype(jnp.bfloat16)
    return (updated, new_state)


def solution(mesh):
    placed = (
        P("ep", "tp"),
        P("ep", None),
        P("ep", None),
        P(None, "ep", "tp"),
        P(),
        P(None, "tp"),
        P("tp", None),
        P("tp", None),
        P("tp"),
        P(None, "tp", None, None),
        P(None, "tp", None, None),
        P("tp"),
        P(),
        P(None, "tp"),
        P(),
        P("ep", None, "tp"),
        P("ep", None, "tp"),
        P("ep", "tp", None),
    )
    return jax.shard_map(
        local,
        mesh=mesh,
        in_specs=placed,
        out_specs=(P("ep", "tp"), P(None, "ep", "tp")),
        check_vma=False,
    )
```

profile of v0, /device:TPU:0, one launch (start us, length us, event | category | flops | bytes accessed | tf_op | source)
XLA Modules:
  0.0 142.8 jit_solution(5299573635172329932)
XLA Ops:
  7.2 0.0 copy-start
  7.2 0.0 all-gather.2.cloned.1.call-start
  7.2 0.9 copy.102
  8.1 0.1 eq.43
  8.2 0.1 eq.39
  8.4 0.0 copy-start.3
  8.4 2.5 %all_gather.9 = bf16[64,2048]{1,0:T(8,128)(2,1)S(1)} all-gather(bf16[64,1024]{1,0:T(8,128)(2,1)} %param.18), channel_id=1, replica_groups=mesh['ep'=16,'tp'=2] {'tp'}, dimensions={1}, use_global_device_ids=true | all-gather | bytes 393216 | tf_op jit(solution)/shard_map/all_gather | solution.py:101
  10.8 0.2 fusion.32
  11.0 2.1 %convolution_convert_fusion.1 = bf16[64,512]{1,0:T(8,128)(2,1)S(1)} fusion(bf16[2048,512]{1,0:T(8,128)(2,1)} %param.23, bf16[64,2048]{1,0:T(8,128)(2,1)S(1)} %all_gather.9, f32[2048]{0:T(1024)} %param.22, f32[64]{0:T(128)S(1)} %add_rsqrt_fusion.2), kind=kOutput, calls=%fused_computation.23 | convolution fusion | flops 134774784 | bytes 2433280 | tf_op jit(solution)/shard_map/dot_general | solution.py:103
  13.1 0.1 copy.93
  13.3 0.0 copy-done.3
  13.3 1.0 fusion.83
  14.3 1.4 copy.91
  15.7 2.4 %copy.92 = f32[1,64,2048]{1,2,0:T(8,128)} copy(f32[1,64,2048]{2,1,0:T(8,128)} %get-tuple-element.3) | data formatting | bytes 1048576 | tf_op jit(solution)/shard_map/slice | solution.py:52
  18.1 0.0 copy-done.8
  18.1 0.0 copy-done.9
  18.1 0.0 copy-done.15
  18.1 0.2 add_divide_fusion
  18.2 0.0 copy-start.1
  18.3 0.0 copy-start.4
  18.3 4.0 %fusion.19 = f32[64,32,64]{0,2,1:T(8,128)} fusion(bf16[64,32,16]{0,2,1:T(8,128)(2,1)S(1)} %bitcast.123, f32[64,32,64]{0,2,1:T(8,128)S(1)} %bitcast.115, f32[64,32,64]{0,2,1:T(8,128)} %bitcast.117, f32[32,64]{1,0:T(8,128)S(1)} %get-tuple-element.7, f32[32,64]{1,0:T(8,128)S(1)} %get-tuple-element.5, f32[2,32,64,16]{2,3,1,0:T(8,128)} %param.27, ...), kind=kOutput, calls=%fused_computation.16 | convolution fusion | flops 25788416 | bytes 1933312 | tf_op jit(solution)/shard_map/sgc,gpc->sgp/dot_general | solution.py:50
  22.3 0.0 copy-done.1
  22.3 2.4 %fusion.18 = f32[64,32,64]{0,2,1:T(8,128)} fusion(bf16[64,32,16]{0,2,1:T(8,128)(2,1)S(1)} %bitcast.124, f32[64,32,64]{0,2,1:T(8,128)S(1)} %bitcast.118, f32[64,32,64]{0,2,1:T(8,128)S(1)} %bitcast.116, f32[32,64]{1,0:T(8,128)S(1)} %get-tuple-element.7, f32[32,64]{1,0:T(8,128)S(1)} %get-tuple-element.5, f32[2,32,64,16]{2,3,1,0:T(8,128)S(1)} %copy-done.4, ...), kind=kOutput, calls=%fused_computation.15 | convolution fusion | flops 25788416 | bytes 1933312 | tf_op jit(solution)/shard_map/sgc,gpc->sgp/dot_general | solution.py:49
  24.7 0.1 mul.286
  24.8 0.6 reduce-window.6
  25.4 0.2 slice_reduce_fusion
  25.6 0.1 fusion.76
  25.7 0.6 copy-done.10
  26.3 0.1 reduce_sum.52
  26.4 0.6 broadcast_multiply_fusion
  27.0 0.1 copy.106
  27.1 0.7 fusion.35
  27.8 2.3 %fusion.46 = f32[32,64,16]{1,2,0:T(8,128)S(1)} fusion(f32[64,32,64]{0,2,1:T(8,128)} %fusion.18, f32[2,32,16,64]{3,2,1,0:T(8,128)} %param.28), kind=kOutput, calls=%fused_computation.47 | convolution fusion | flops 25165824 | bytes 1441792 | tf_op jit(solution)/shard_map/dfk,idk->idf/dot_general | solution.py:56
  30.1 0.0 copy-done.5
  30.1 1.6 %multiply_reduce_fusion.2 = (f32[64]{0:T(128)}, f32[64,32,16]{0,2,1:T(8,128)S(1)}) fusion(bf16[64,32,16]{0,2,1:T(8,128)(2,1)S(1)} %bitcast.125, f32[32,16]{1,0:T(8,128)S(1)} %mul.286, f32[32,64,16]{1,2,0:T(8,128)S(1)} %fusion.46, f32[64,32,64]{0,2,1:T(8,128)S(1)} %copy-done.2, f32[2,32,16,64]{3,2,1,0:T(8,128)S(1)} %copy-done.5), kind=kOutput, calls=%fused_computation.58 | convolution fusion | flops 25690048 | bytes 1851648 | tf_op jit(solution)/shard_map/dfk,idk->idf/dot_general | solution.py:57
  31.7 2.6 %psum.14 = f32[64]{0:T(128)S(1)} all-reduce(f32[64]{0:T(128)} %get-tuple-element.10), channel_id=1, replica_groups=mesh['ep'=16,'tp'=2] {'tp'}, use_global_device_ids=true, to_apply=%region_2.0 | all-reduce | flops 64 | bytes 512 | tf_op jit(solution)/shard_map/psum | solution.py:118
  34.3 0.1 copy.100
  34.4 0.0 copy-start.14
  34.5 0.8 dynamic_slice.6
  35.2 0.1 multiply_convert_fusion.3
  35.3 1.9 %all_gather.10 = bf16[64,1024]{1,0:T(8,128)(2,1)S(1)} all-gather(bf16[64,512]{1,0:T(8,128)(2,1)S(1)} %multiply_convert_fusion.3), channel_id=1, replica_groups=mesh['ep'=16,'tp'=2] {'tp'}, dimensions={1}, use_global_device_ids=true | all-gather | bytes 196608 | tf_op jit(solution)/shard_map/all_gather | solution.py:122
  37.2 1.5 %multiply_reduce_fusion.1 = (f32[64]{0:T(128)S(1)}, f32[64,1024]{1,0:T(8,128)S(1)}) fusion(bf16[64,1024]{1,0:T(8,128)(2,1)S(1)} %all_gather.10, bf16[1024,1024]{1,0:T(8,128)(2,1)S(1)} %copy-done, bf16[64,1024]{1,0:T(8,128)(2,1)} %param.18), kind=kOutput, calls=%fused_computation.57 | convolution fusion | flops 134610880 | bytes 2621696 | tf_op jit(solution)/shard_map/dot_general | solution.py:124
  38.7 2.5 %psum.15 = f32[64]{0:T(128)S(1)} all-reduce(f32[64]{0:T(128)S(1)} %get-tuple-element.12), channel_id=1, replica_groups=mesh['ep'=16,'tp'=2] {'tp'}, use_global_device_ids=true, to_apply=%region_8.9 | all-reduce | flops 64 | bytes 512 | tf_op jit(solution)/shard_map/psum | solution.py:139
  41.2 0.4 convolution_convert_fusion
  41.7 29.7 %all_to_all.10 = bf16[16,1,24,1024]{3,2,1,0:T(8,128)(2,1)} all-to-all(bf16[16,1,24,1024]{3,2,1,0:T(8,128)(2,1)S(1)} %bitcast.122), channel_id=1, replica_groups=mesh['ep'=16,'tp'=2] {'ep'}, dimensions={0} | all-to-all | bytes 1572864 | tf_op jit(solution)/shard_map/all_to_all | solution.py:146
  71.4 0.0 all-gather.2.cloned.1.call-update
  71.4 0.2 reduce-scatter.2.cloned.1.call-start
  71.6 7.5 %all-gather.2.cloned.1.call-done = bf16[16,1,24,2048]{3,2,0,1:T(8,128)(2,1)} async-done(((bf16[16,1,24,1024]{3,2,0,1:T(8,128)(2,1)}), bf16[16,1,24,2048]{3,2,0,1:T(8,128)(2,1)}) %all-gather.2.cloned.1.call-update) | async-done | bytes 1572880 | tf_op jit(solution)/shard_map/all_gather | solution.py:145
  79.1 5.6 %fusion.2 = f32[16,24,1024]{2,1,0:T(8,128)} fusion(bf16[1,2048,1024]{2,1,0:T(8,128)(2,1)} %param.33, bf16[16,1,24,2048]{3,2,0,1:T(8,128)(2,1)} %all-gather.2.cloned.1.call-done), kind=kOutput, calls=%fused_computation.3 | convolution fusion | flops 1610612736 | bytes 7340032 | tf_op jit(solution)/shard_map/necd,edf->necf/dot_general | solution.py:151
  84.7 9.3 %fusion.9 = bf16[16,1,24,2048]{3,2,0,1:T(8,128)(2,1)} fusion(bf16[1,1024,2048]{2,1,0:T(8,128)(2,1)} %param.35, f32[16,24,1024]{2,1,0:T(8,128)} %fusion.2, bf16[1,2048,1024]{2,1,0:T(8,128)(2,1)} %param.34, bf16[16,1,24,2048]{3,2,0,1:T(8,128)(2,1)} %all-gather.2.cloned.1.call-done), kind=kOutput, calls=%fused_computation.8 | convolution fusion | flops 3225944064 | bytes 13107200 | tf_op jit(solution)/shard_map/necf,efd->necd/dot_general | solution.py:159
  94.0 0.0 reduce-scatter.2.cloned.1.call-update
  94.0 10.3 %reduce-scatter.2.cloned.1.call-done = bf16[16,1,24,1024]{3,2,0,1:T(8,128)(2,1)} async-done(((bf16[16,1,24,2048]{3,2,0,1:T(8,128)(2,1)}), bf16[16,1,24,1024]{3,2,0,1:T(8,128)(2,1)}) %reduce-scatter.2.cloned.1.call-update) | async-done | bytes 786448 | tf_op jit(solution)/shard_map/reduce_scatter | solution.py:163
  104.3 6.9 %all-to-all-start.1 = ((bf16[16,1,24,1024]{3,2,1,0:T(8,128)(2,1)}), bf16[16,1,24,1024]{3,2,1,0:T(8,128)(2,1)S(1)}, u32[]{:S(2)}, u32[]{:S(2)}) async-start(bf16[16,1,24,1024]{3,2,1,0:T(8,128)(2,1)} %bitcast.127), calls=%async_computation.2 | async-start | bytes 1572864 | tf_op jit(solution)/shard_map/all_to_all | solution.py:166
  111.2 0.1 mul.326
  111.3 0.1 copy.101
  111.4 2.3 %copy.111 = f32[1,64,2048]{2,1,0:T(8,128)} copy(f32[1,64,2048]{1,2,0:T(8,128)} %bitcast.120) | data formatting | bytes 1048576 | tf_op jit(solution)/shard_map/stack;reshape | solution.py:65
  113.7 2.4 %copy.110 = f32[1,64,2048]{2,1,0:T(8,128)} copy(f32[1,64,2048]{1,2,0:T(8,128)} %bitcast.119) | data formatting | bytes 1048576 | tf_op jit(solution)/shard_map/stack;reshape | solution.py:65
  116.1 0.0 copy-done.11
  116.1 2.3 %pad_maximum_fusion = f32[2,64,2048]{2,1,0:T(8,128)} fusion(f32[1,64,2048]{2,1,0:T(8,128)} %copy.111, f32[1,64,2048]{2,1,0:T(8,128)} %copy.110), kind=kLoop, calls=%fused_computation.24 | loop fusion | flops 262144 | bytes 2097152 | tf_op jit(solution)/shard_map/stack | solution.py:65
  118.4 12.8 %all-to-all-done.1 = bf16[16,1,24,1024]{3,2,1,0:T(8,128)(2,1)S(1)} async-done(((bf16[16,1,24,1024]{3,2,1,0:T(8,128)(2,1)}), bf16[16,1,24,1024]{3,2,1,0:T(8,128)(2,1)S(1)}, u32[]{:S(2)}, u32[]{:S(2)}) %all-to-all-start.1) | async-done | bytes 786464 | tf_op jit(solution)/shard_map/all_to_all | solution.py:166
  131.2 2.0 %gather_fusion = bf16[256,1024]{1,0:T(8,128)(2,1)} fusion(bf16[384,1024]{1,0:T(8,128)(2,1)S(1)} %bitcast.114, s32[1024]{0:T(1024)S(1)} %pad_clamp_fusion), kind=kCustom, calls=%fused_computation | custom fusion | bytes 1049600 | tf_op jit(solution)/shard_map/gather | solution.py:168
  133.1 1.4 reshape.136
  134.5 0.7 multiply_reduce_fusion
  135.2 0.7 add_convert_fusion
  (28 shorter events, 0.1 us)
Async XLA Ops:
  7.2 30.1 %copy-start = (bf16[1024,1024]{1,0:T(8,128)(2,1)S(1)}, bf16[1024,1024]{1,0:T(8,128)(2,1)}, u32[]{:S(2)}) copy-start(bf16[1024,1024]{1,0:T(8,128)(2,1)} %param.31) | copy-start | bytes 6291460
  7.2 71.9 %all-gather.2.cloned.1.call-start = ((), (), s32[]{:S(2)}) async-start(), calls=%async_computation.3 | async-start | bytes 2359296 | tf_op jit(solution)/shard_map/all_gather | solution.py:145
  8.4 4.9 %copy-start.3 = (f32[2,64,2048]{2,1,0:T(8,128)S(1)}, f32[2,64,2048]{2,1,0:T(8,128)}, u32[]{:S(2)}) copy-start(f32[2,64,2048]{2,1,0:T(8,128)} %param.21) | copy-start | bytes 3145732
  14.3 3.8 %copy-start.8 = (f32[32,64]{1,0:T(8,128)S(1)}, f32[32,64]{1,0:T(8,128)}, u32[]{:S(2)}) copy-start(f32[32,64]{1,0:T(8,128)} %param.25) | copy-start | bytes 24580
  14.3 3.8 %copy-start.9 = (f32[32,64]{1,0:T(8,128)S(1)}, f32[32,64]{1,0:T(8,128)}, u32[]{:S(2)}) copy-start(f32[32,64]{1,0:T(8,128)} %param.24) | copy-start | bytes 24580
  14.3 3.8 %copy-start.15 = (f32[32]{0:T(128)S(1)}, f32[32]{0:T(128)}, u32[]{:S(2)}) copy-start(f32[32]{0:T(128)} %param.26) | copy-start | bytes 388
  18.2 4.0 %copy-start.1 = (f32[1,64,2048]{1,2,0:T(8,128)S(1)}, f32[1,64,2048]{1,2,0:T(8,128)}, u32[]{:S(2)}) copy-start(f32[1,64,2048]{1,2,0:T(8,128)} %copy.92) | copy-start | bytes 1572868
  18.3 4.0 %copy-start.4 = (f32[2,32,64,16]{2,3,1,0:T(8,128)S(1)}, f32[2,32,64,16]{2,3,1,0:T(8,128)}, u32[]{:S(2)}) copy-start(f32[2,32,64,16]{2,3,1,0:T(8,128)} %param.27) | copy-start | bytes 786436
  22.3 2.4 %copy-start.12 = (f32[512]{0:T(512)S(1)}, f32[512]{0:T(512)}, u32[]{:S(2)}) copy-start(f32[512]{0:T(512)} %param.29) | copy-start | bytes 6148
  24.7 5.4 %copy-start.2 = (f32[64,32,64]{0,2,1:T(8,128)S(1)}, f32[64,32,64]{0,2,1:T(8,128)}, u32[]{:S(2)}) copy-start(f32[64,32,64]{0,2,1:T(8,128)} %fusion.19) | copy-start | bytes 1572868
  25.7 0.6 copy-start.10
  27.1 3.0 %copy-start.5 = (f32[2,32,16,64]{3,2,1,0:T(8,128)S(1)}, f32[2,32,16,64]{3,2,1,0:T(8,128)}, u32[]{:S(2)}) copy-start(f32[2,32,16,64]{3,2,1,0:T(8,128)} %param.28) | copy-start | bytes 786436
  34.4 6.8 %copy-start.14 = (f32[2048]{0:T(1024)S(1)}, f32[2048]{0:T(1024)}, u32[]{:S(2)}) copy-start(f32[2048]{0:T(1024)} %param.32) | copy-start | bytes 24580
  34.4 6.8 %copy-start.7 = (pred[384,64]{0,1:T(8,128)(4,1)S(1)}, pred[384,64]{0,1:T(8,128)(4,1)}, u32[]{:S(2)}) copy-start(pred[384,64]{0,1:T(8,128)(4,1)} %fusion.35) | copy-start | bytes 73732
  71.4 32.9 %reduce-scatter.2.cloned.1.call-start = ((), (), s32[]{:S(2)}) async-start(), calls=%async_computation.4 | async-start | bytes 2359296 | tf_op jit(solution)/shard_map/reduce_scatter | solution.py:163
  93.9 17.2 %copy-start.6 = (s32[64,4]{1,0:T(8,128)S(1)}, s32[64,4]{1,0:T(8,128)}, u32[]{:S(2)}) copy-start(s32[64,4]{1,0:T(8,128)} %get-tuple-element.8) | copy-start | bytes 3076
  93.9 17.3 %copy-start.13 = (f32[64,4]{0,1:T(4,128)S(1)}, f32[64,4]{0,1:T(4,128)}, u32[]{:S(2)}) copy-start(f32[64,4]{0,1:T(4,128)} %param.20) | copy-start | bytes 3076
  104.3 26.9 %all-to-all-start.1 = ((bf16[16,1,24,1024]{3,2,1,0:T(8,128)(2,1)}), bf16[16,1,24,1024]{3,2,1,0:T(8,128)(2,1)S(1)}, u32[]{:S(2)}, u32[]{:S(2)}) async-start(bf16[16,1,24,1024]{3,2,1,0:T(8,128)(2,1)} %bitcast.127), calls=%async_computation.2 | async-start | bytes 1572864 | tf_op jit(solution)/shard_map/all_to_all | solution.py:166
  111.4 4.7 %copy-start.11 = (s32[256]{0:T(256)S(1)}, s32[256]{0:T(256)}, u32[]{:S(2)}) copy-start(s32[256]{0:T(256)} %copy-done.10) | copy-start | bytes 3076
Sparse Core Ops, SparseCore 0:
  71.5 7.5 all-gather.1
  94.1 10.1 reduce-scatter.1
where the time goes:
time: 143 us
  blocking collectives  39.2 us (27%)
  waiting for transfers between devices  30.6 us (21%)
  matrix products  29.2 us (20%)
  local copies, waits for them, and re-layouts  16.3 us (11%)
  between operations  14.3 us (10%)
  starting transfers between devices  7.17 us (5%)
  other arithmetic  6.17 us (4%)
    all_to_all x1, blocking collectives, local(): lax.all_to_all(buffer, 'ep', split_axis=0, concat_axis=0, tiled=True)  29.7 us
    all_to_all x1, waiting for transfers between devices, local(): lax.all_to_all(summed, 'ep', split_axis=0, concat_axis=0, tiled=True)  12.8 us
    reduce_scatter x1, waiting for transfers between devices, local(): lax.psum_scatter(partial_value.astype(jnp.bfloat16), 'tp', scatter_dimens...  10.3 us
    dot_general x1, matrix products, local(): jnp.einsum('necf,efd->necd', activation, w_down, preferred_element_type=j...  9.25 us
    all_gather x1, waiting for transfers between devices, local(): lax.all_gather(lax.all_to_all(buffer, 'ep', split_axis=0, concat_axis=0,...  7.47 us
    all_to_all x1, starting transfers between devices, local(): lax.all_to_all(summed, 'ep', split_axis=0, concat_axis=0, tiled=True)  6.91 us
    dot_general x1, matrix products, local(): jnp.einsum('necd,edf->necf', arrived, w_gate, preferred_element_type=jnp....  5.59 us
    psum x2, blocking collectives, local(): total_sq = lax.psum(jnp.sum(own_half * own_half, axis=1), 'tp')  5.08 us
  transfers between devices with their start and end apart: 3, of which 3 were waited for; matrix products, arithmetic and copies ran while one was open for 5% of the time, Pallas kernels for 0%

commit v1 on v0

v1 whole, which is shorter than its diff:
```python
import functools

import jax
import jax.numpy as jnp
from jax import lax
from jax.experimental import pallas as pl
from jax.experimental.pallas import tpu as pltpu
from jax.sharding import PartitionSpec as P

epsilon = 1e-06
clamp_limit = 7.0
swish_alpha = 1.702
f32, bf16 = jnp.float32, jnp.bfloat16
NN = (((1,), (0,)), ((), ()))
NT = (((1,), (1,)), ((), ()))
TN = (((0,), (0,)), ((), ()))


def mm(a, b, dims=NN):
    return lax.dot_general(a, b, dims, preferred_element_type=f32)


def split(values):
    high = values.astype(bf16)
    return high, (values - high.astype(f32)).astype(bf16)


def flat_row(table):
    groups, width = table.shape
    tiled = jnp.concatenate([table] * groups, axis=1)
    lane = lax.broadcasted_iota(jnp.int32, tiled.shape, 1)
    first = lax.broadcasted_iota(jnp.int32, tiled.shape, 0) * width
    own = (lane >= first) & (lane < first + width)
    return jnp.sum(jnp.where(own, tiled, 0.0), axis=0, keepdims=True)


def spread(table, count):
    _, per_group, width = table.shape
    tiled = jnp.concatenate([table] * count, axis=2)
    lane = lax.broadcasted_iota(jnp.int32, tiled.shape, 2)
    first = lax.broadcasted_iota(jnp.int32, tiled.shape, 0) * width
    own = (lane >= first) & (lane < first + width)
    return jnp.where(own, tiled, 0.0).reshape(count * per_group, count * width)


def mixer_kernel(
    own_ref,
    other_ref,
    state_ref,
    gain_ref,
    proj_ref,
    decay_ref,
    freq_ref,
    step_ref,
    map_ref,
    out_ref,
    skip_ref,
    act_ref,
    new_ref,
):
    first = lax.axis_index("tp") == 0
    own, other = own_ref[...].astype(f32), other_ref[...].astype(f32)
    half = own.shape[1]
    low, high = jnp.where(first, own, other), jnp.where(first, other, own)
    total = jnp.sum(low * low, axis=1, keepdims=True) + jnp.sum(high * high, axis=1, keepdims=True)
    scale = lax.rsqrt(total / (2 * half) + epsilon)
    gain = gain_ref[...]
    low = (low * scale * gain[:, :half]).astype(bf16)
    high = (high * scale * gain[:, half:]).astype(bf16)
    channels = (mm(low, proj_ref[:half, :]) + mm(high, proj_ref[half:, :])).astype(bf16)

    groups, width = decay_ref.shape
    per_group = map_ref.shape[2]
    step = step_ref[...]
    square = jnp.broadcast_to(step, (groups, groups))
    diagonal = lax.broadcasted_iota(jnp.int32, square.shape, 0) == lax.broadcasted_iota(
        jnp.int32, square.shape, 1
    )
    step = jnp.sum(jnp.where(diagonal, square, 0.0), axis=1, keepdims=True)
    rate, freq = -decay_ref[...], freq_ref[...]
    magnitude = jnp.exp(rate * step)
    phase = freq * step
    bar_real, bar_imag = magnitude * jnp.cos(phase), magnitude * jnp.sin(phase)
    inverse = 1.0 / (rate * rate + freq * freq)
    shifted = bar_real - 1.0
    coef_real = ((shifted * rate + bar_imag * freq) * inverse)[:, None, :]
    coef_imag = ((bar_imag * rate - shifted * freq) * inverse)[:, None, :]
    map_real = coef_real * map_ref[0] - coef_imag * map_ref[1]
    map_imag = coef_real * map_ref[1] + coef_imag * map_ref[0]
    bar_real, bar_imag = flat_row(bar_real), flat_row(bar_imag)

    count = max(1, min(groups, 128 // per_group))
    lanes, columns = count * width, count * per_group
    for block in range(groups // count):
        held = slice(block * count, (block + 1) * count)
        wide = slice(block * lanes, (block + 1) * lanes)
        narrow = slice(block * columns, (block + 1) * columns)
        fed = channels[:, narrow]
        real_high, real_low = split(spread(map_real[held], count))
        imag_high, imag_low = split(spread(map_imag[held], count))
        old_real, old_imag = state_ref[0, :, wide], state_ref[1, :, wide]
        turn_real, turn_imag = bar_real[:, wide], bar_imag[:, wide]
        next_real = (
            turn_real * old_real - turn_imag * old_imag + (mm(fed, real_high) + mm(fed, real_low))
        )
        next_imag = (
            turn_real * old_imag + turn_imag * old_real + (mm(fed, imag_high) + mm(fed, imag_low))
        )
        new_ref[0, :, wide] = next_real
        new_ref[1, :, wide] = next_imag
        a_high, a_low = split(spread(out_ref[0, held], count))
        b_high, b_low = split(spread(-out_ref[1, held], count))
        r_high, r_low = split(next_real)
        i_high, i_low = split(next_imag)
        mixed = (mm(r_high, a_high, NT) + mm(i_high, b_high, NT)) + (
            mm(r_low, a_high, NT)
            + mm(r_high, a_low, NT)
            + mm(i_low, b_high, NT)
            + mm(i_high, b_low, NT)
        )
        mixed = mixed + skip_ref[:, narrow] * fed.astype(f32)
        act_ref[:, narrow] = jax.nn.gelu(mixed).astype(bf16)


def slots_of(ids, experts, capacity):
    rows = ids.shape[1]
    expert = lax.broadcasted_iota(jnp.int32, (experts, rows), 0)
    named = jnp.zeros((experts, rows), f32)
    for k in range(ids.shape[0]):
        named = named + (ids[k : k + 1, :] == expert).astype(f32)
    earlier = lax.broadcasted_iota(jnp.int32, (rows, rows), 0) < lax.broadcasted_iota(
        jnp.int32, (rows, rows), 1
    )
    rank = mm(named.astype(bf16), earlier.astype(f32).astype(bf16))
    rank = jnp.where(named > 0.0, rank, -1.0).astype(jnp.int32)
    slot = lax.broadcasted_iota(jnp.int32, (experts, capacity, rows), 1)
    return rank[:, None, :] == slot


def dispatch_kernel(capacity, experts, own_ref, other_ref, gain_ref, proj_ref, residual_ref, ids_ref, mid_ref, sent_ref):
    first = lax.axis_index("tp") == 0
    own, other = own_ref[...].astype(f32), other_ref[...].astype(f32)
    half = own.shape[1]
    low, high = jnp.where(first, own, other), jnp.where(first, other, own)
    total = jnp.sum(low * low, axis=1, keepdims=True) + jnp.sum(high * high, axis=1, keepdims=True)
    scale = lax.rsqrt(total / (2 * half) + epsilon)
    gain = gain_ref[...]
    low = (low * scale * gain[:, :half]).astype(bf16)
    high = (high * scale * gain[:, half:]).astype(bf16)
    product = mm(low, proj_ref[:half, :]) + mm(high, proj_ref[half:, :])
    mid = (residual_ref[...].astype(f32) + product).astype(bf16)
    mid_ref[...] = mid
    rows = mid.shape[0]
    table = slots_of(ids_ref[...], experts, capacity).astype(f32)
    table = table.reshape(experts * capacity, rows).astype(bf16)
    sent_ref[...] = mm(table, mid).astype(bf16)


def expert_kernel(own_ref, other_ref, gain_ref, gate_ref, up_ref, down_ref, keep_ref, send_ref, rows_ref, sum_ref):
    step = pl.program_id(0)
    half = own_ref.shape[1]
    tp = lax.axis_index("tp")

    @pl.when(step == 0)
    def _():
        own, other = own_ref[...].astype(f32), other_ref[...].astype(f32)
        low, high = jnp.where(tp == 0, own, other), jnp.where(tp == 0, other, own)
        total = jnp.sum(low * low, axis=1, keepdims=True) + jnp.sum(
            high * high, axis=1, keepdims=True
        )
        scale = lax.rsqrt(total / (2 * half) + epsilon)
        gain = gain_ref[...]
        rows_ref[:, :half] = (low * scale * gain[:, :half]).astype(bf16)
        rows_ref[:, half:] = (high * scale * gain[:, half:]).astype(bf16)

    rows = rows_ref[...]
    gated = jnp.minimum(mm(rows, gate_ref[...]), clamp_limit)
    lifted = jnp.clip(mm(rows, up_ref[...]), -clamp_limit, clamp_limit) + 1.0
    active = (lifted * gated * jax.nn.sigmoid(swish_alpha * gated)).astype(bf16)
    product = mm(active, down_ref[...])

    @pl.when(step == 0)
    def _():
        sum_ref[...] = product

    @pl.when(step > 0)
    def _():
        sum_ref[...] += product

    @pl.when(step == pl.num_programs(0) - 1)
    def _():
        mine = pl.multiple_of(tp * half, half)
        theirs = pl.multiple_of((1 - tp) * half, half)
        keep_ref[...] = sum_ref[:, pl.ds(mine, half)].astype(bf16)
        send_ref[...] = sum_ref[:, pl.ds(theirs, half)].astype(bf16)


def combine_kernel(capacity, experts, ids_ref, weights_ref, mid_ref, back_ref, out_ref):
    ids = ids_ref[...]
    rows = ids.shape[1]
    mask = slots_of(ids, experts, capacity)
    expert = lax.broadcasted_iota(jnp.int32, (experts, rows), 0)
    weight = jnp.zeros((experts, rows), f32)
    for k in range(ids.shape[0]):
        weight = weight + jnp.where(ids[k : k + 1, :] == expert, weights_ref[k : k + 1, :], 0.0)
    table = jnp.where(mask, weight[:, None, :], 0.0).reshape(experts * capacity, rows)
    high, low = split(table)
    back = back_ref[...]
    total = mm(high, back, TN) + mm(low, back, TN)
    out_ref[...] = (mid_ref[...].astype(f32) + total).astype(bf16)


def local(
    residual,
    route_ids,
    route_weights,
    carried_state,
    mix_gain,
    in_proj,
    decay_rate,
    frequency,
    step_size,
    input_map,
    output_matrix,
    passthrough_scale,
    out_gain,
    out_proj,
    ffn_gain,
    w_gate,
    w_up,
    w_down,
):
    rows, half = residual.shape
    top = route_ids.shape[1]
    peers = lax.axis_size("ep")
    experts = w_gate.shape[0] * peers
    capacity = max(2, 3 * rows * top // (2 * experts))
    capacity = -(-capacity // 8) * 8
    channel_half = in_proj.shape[1]
    hidden = w_gate.shape[2]
    swap = [(0, 1), (1, 0)]
    ids, weights = route_ids.T, route_weights.T
    params = pltpu.CompilerParams(vmem_limit_bytes=48 * 1024 * 1024)

    other = lax.ppermute(residual, "tp", swap)
    active, new_state = pl.pallas_call(
        mixer_kernel,
        out_shape=(
            jax.ShapeDtypeStruct((rows, channel_half), bf16),
            jax.ShapeDtypeStruct(carried_state.shape, f32),
        ),
        compiler_params=params,
        name="mixer",
    )(
        residual,
        other,
        carried_state,
        mix_gain.reshape(1, -1),
        in_proj,
        decay_rate,
        frequency,
        step_size.reshape(1, -1),
        jnp.swapaxes(input_map, 2, 3),
        output_matrix,
        passthrough_scale.reshape(1, -1),
    )
    other = lax.ppermute(active, "tp", swap)
    slots = experts * capacity
    mid, sent = pl.pallas_call(
        functools.partial(dispatch_kernel, capacity, experts),
        out_shape=(
            jax.ShapeDtypeStruct((rows, half), bf16),
            jax.ShapeDtypeStruct((slots, half), bf16),
        ),
        compiler_params=params,
        name="dispatch",
    )(active, other, out_gain.reshape(1, -1), out_proj, residual, ids)

    def exchange(values):
        values = values.reshape(peers, slots // peers, half)
        values = lax.all_to_all(values, "ep", split_axis=0, concat_axis=0, tiled=True)
        return values.reshape(slots, half)

    arrived = exchange(sent)
    other = lax.ppermute(arrived, "tp", swap)
    tiles = max(1, hidden // 256)
    tile = hidden // tiles
    keep, send = pl.pallas_call(
        expert_kernel,
        grid=(tiles,),
        in_specs=[
            pl.BlockSpec((slots, half), lambda j: (0, 0)),
            pl.BlockSpec((slots, half), lambda j: (0, 0)),
            pl.BlockSpec((1, 2 * half), lambda j: (0, 0)),
            pl.BlockSpec((None, 2 * half, tile), lambda j: (0, 0, j)),
            pl.BlockSpec((None, 2 * half, tile), lambda j: (0, 0, j)),
            pl.BlockSpec((None, tile, 2 * half), lambda j: (0, j, 0)),
        ],
        out_specs=(
            pl.BlockSpec((slots, half), lambda j: (0, 0)),
            pl.BlockSpec((slots, half), lambda j: (0, 0)),
        ),
        out_shape=(jax.ShapeDtypeStruct((slots, half), bf16),) * 2,
        scratch_shapes=[pltpu.VMEM((slots, 2 * half), bf16), pltpu.VMEM((slots, 2 * half), f32)],
        compiler_params=params,
        name="experts",
    )(arrived, other, ffn_gain.reshape(1, -1), w_gate, w_up, w_down)
    other = lax.ppermute(send, "tp", swap)
    back = exchange((keep.astype(f32) + other.astype(f32)).astype(bf16))
    updated = pl.pallas_call(
        functools.partial(combine_kernel, capacity, experts),
        out_shape=jax.ShapeDtypeStruct((rows, half), bf16),
        compiler_params=params,
        name="combine",
    )(ids, weights, mid, back)
    return updated, new_state


def solution(mesh):
    placed = (
        P("ep", "tp"),
        P("ep", None),
        P("ep", None),
        P(None, "ep", "tp"),
        P(),
        P(None, "tp"),
        P("tp", None),
        P("tp", None),
        P("tp"),
        P(None, "tp", None, None),
        P(None, "tp", None, None),
        P("tp"),
        P(),
        P(None, "tp"),
        P(),
        P("ep", None, "tp"),
        P("ep", None, "tp"),
        P("ep", "tp", None),
    )
    return jax.shard_map(
        local,
        mesh=mesh,
        in_specs=placed,
        out_specs=(P("ep", "tp"), P(None, "ep", "tp")),
        check_vma=False,
    )
```

time: 143 us -> 88 us (0.62)
  matrix products: 29.2 us -> 0 us
  waiting for transfers between devices: 30.6 us -> 6.53 us
  Pallas kernels: 0 us -> 15.1 us
  blocking collectives: 39.2 us -> 54.3 us
  between operations: 14.3 us -> 0.68 us
  local copies, waits for them, and re-layouts: 16.3 us -> 9.29 us
  starting transfers between devices: 7.17 us -> 1.13 us
  other arithmetic: 6.17 us -> 0.3 us
    dot_general x9 -> x0, matrix products: 29.2 us -> none  [the longest x1 9.25 us: local(): jnp.einsum('necf,efd->necd', activation, w_down, preferred_element_type=j...]
    all_to_all x1 -> x2, blocking collectives: 29.7 us -> 54.3 us  [exchange(): lax.all_to_all(values, 'ep', split_axis=0, concat_axis=0, tiled=True)]
    pallas_call x0 -> x4, Pallas kernels: none -> 15.1 us  [the longest x1 10 us: local(): pl.pallas_call(expert_kernel, grid=(tiles,), in_specs=[pl.BlockSpec((slot...]
    all_to_all x1 -> x0, waiting for transfers between devices: 12.8 us -> none  [local(): lax.all_to_all(summed, 'ep', split_axis=0, concat_axis=0, tiled=True)]
    reduce_scatter x1 -> x0, waiting for transfers between devices: 10.3 us -> none  [local(): lax.psum_scatter(partial_value.astype(jnp.bfloat16), 'tp', scatter_dimens...]
    unnamed x34 -> x30, local copies, waits for them, and re-layouts: 1.67 us -> 9.29 us
    all_gather x1 -> x0, waiting for transfers between devices: 7.47 us -> none  [local(): lax.all_gather(lax.all_to_all(buffer, 'ep', split_axis=0, concat_axis=0,...]
    all_to_all x1 -> x0, starting transfers between devices: 6.91 us -> none  [local(): lax.all_to_all(summed, 'ep', split_axis=0, concat_axis=0, tiled=True)]
  transfers between devices with their start and end apart: 3 -> 4, of which waited for: 3 -> 4; matrix products, arithmetic and copies ran while one was open for 5% -> 0% of each run, Pallas kernels for 0% -> 0%
where the time goes in v1:
time: 88 us; the launch traced here: 87.4 us
  blocking collectives  54.3 us (62%)
  Pallas kernels  15.1 us (17%)
  local copies, waits for them, and re-layouts  9.29 us (11%)
  waiting for transfers between devices  6.53 us (7%)
  starting transfers between devices  1.13 us (1%)
    all_to_all x2, blocking collectives, exchange(): lax.all_to_all(values, 'ep', split_axis=0, concat_axis=0, tiled=True)  54.3 us
    pallas_call x1, Pallas kernels, local(): pl.pallas_call(expert_kernel, grid=(tiles,), in_specs=[pl.BlockSpec((slot...  10 us
    unnamed x30, local copies, waits for them, and re-layouts  9.29 us
    pallas_call x1, Pallas kernels, local(): pl.pallas_call(mixer_kernel, out_shape=(jax.ShapeDtypeStruct((rows, chann...  2.94 us
    ppermute x1, waiting for transfers between devices, local(): other = lax.ppermute(arrived, 'tp', swap)  2.28 us
    ppermute x1, waiting for transfers between devices, local(): other = lax.ppermute(send, 'tp', swap)  2.15 us
  transfers between devices with their start and end apart: 4, of which 4 were waited for; matrix products, arithmetic and copies ran while one was open for 0% of the time, Pallas kernels for 0%

profile of v1, /device:TPU:0, one launch (start us, length us, event | category | flops | bytes accessed | tf_op | source)
XLA Modules:
  0.0 87.4 jit_solution(13074036722164900932)
XLA Ops:
  0.6 0.6 collective-permute-start
  1.2 1.2 %collective-permute-done.other_ref = bf16[64,1024]{1,0:T(8,128)(2,1)S(1)} collective-permute-done((bf16[64,1024]{1,0:T(8,128)(2,1)}, bf16[64,1024]{1,0:T(8,128)(2,1)S(1)}, u32[]{:S(2)}, u32[]{:S(2)}) %collective-permute-start) | collective-permute-done | bytes 131104 | tf_op jit(solution)/shard_map/ppermute | solution.py:245
  2.4 0.0 copy-start
  2.4 1.6 %copy-done = bf16[2048,512]{1,0:T(8,128)(2,1)S(1)} copy-done((bf16[2048,512]{1,0:T(8,128)(2,1)S(1)}, bf16[2048,512]{1,0:T(8,128)(2,1)}, u32[]{:S(2)}) %copy-start) | copy-done | bytes 2097176
  4.0 0.0 copy-start.2
  4.0 1.2 %copy-done.2 = f32[2,64,2048]{2,1,0:T(8,128)S(1)} copy-done((f32[2,64,2048]{2,1,0:T(8,128)S(1)}, f32[2,64,2048]{2,1,0:T(8,128)}, u32[]{:S(2)}) %copy-start.2) | copy-done | bytes 1048600
  5.2 0.0 copy-start.3
  5.2 1.0 %copy-done.3 = f32[2,32,64,16]{2,3,1,0:T(8,128)S(1)} copy-done((f32[2,32,64,16]{2,3,1,0:T(8,128)S(1)}, f32[2,32,64,16]{2,3,1,0:T(8,128)}, u32[]{:S(2)}) %copy-start.3) | copy-done | bytes 262168
  6.2 0.0 copy-start.4
  6.2 1.0 %copy-done.4 = f32[2,32,16,64]{3,2,1,0:T(8,128)S(1)} copy-done((f32[2,32,16,64]{3,2,1,0:T(8,128)S(1)}, f32[2,32,16,64]{3,2,1,0:T(8,128)}, u32[]{:S(2)}) %copy-start.4) | copy-done | bytes 262168
  7.3 0.0 copy-start.5
  7.3 0.9 %copy-done.5 = bf16[64,1024]{1,0:T(8,128)(2,1)S(1)} copy-done((bf16[64,1024]{1,0:T(8,128)(2,1)S(1)}, bf16[64,1024]{1,0:T(8,128)(2,1)}, u32[]{:S(2)}) %copy-start.5) | copy-done | bytes 131096
  8.2 0.0 copy-start.6
  8.2 0.7 copy-done.6
  8.9 0.0 copy-start.7
  8.9 0.7 copy-done.7
  9.6 0.0 copy-start.8
  9.6 0.7 copy-done.8
  10.3 0.0 copy-start.12
  10.3 0.7 copy-done.12
  11.0 0.0 copy-start.14
  11.0 0.7 copy-done.14
  11.7 0.0 copy-start.1
  11.7 0.0 copy-start.10
  11.7 0.0 copy-start.11
  11.7 2.9 %mixer.1 = (bf16[64,512]{1,0:T(8,128)(2,1)S(1)}, f32[2,64,2048]{2,1,0:T(8,128)}) custom-call(bf16[64,1024]{1,0:T(8,128)(2,1)S(1)} %copy-done.5, bf16[64,1024]{1,0:T(8,128)(2,1)S(1)} %collective-permute-done.other_ref, f32[2,64,2048]{2,1,0:T(8,128)S(1)} %copy-done.2, f32[1,2048]{1,0:T(1,128)S(1)} %bitcast.17, bf16[2048,512]{1,0:T(8,128)(2,1)S(1)} %copy-done, ...), custom_call_target="tpu_custom_call" | custom-call | tf_op jit(solution)/shard_map/mixer/pallas_call | solution.py:246
  14.6 0.0 copy-start.9
  14.6 0.4 collective-permute-start.1
  15.0 0.9 %collective-permute-done.1.other_ref = bf16[64,512]{1,0:T(8,128)(2,1)S(1)} collective-permute-done((bf16[64,512]{1,0:T(8,128)(2,1)S(1)}, bf16[64,512]{1,0:T(8,128)(2,1)S(1)}, u32[]{:S(2)}, u32[]{:S(2)}) %collective-permute-start.1) | collective-permute-done | bytes 65568 | tf_op jit(solution)/shard_map/ppermute | solution.py:267
  15.9 0.0 copy-done.1
  15.9 0.0 copy-done.10
  15.9 0.0 copy-done.11
  15.9 0.9 %dispatch.1 = (bf16[64,1024]{1,0:T(8,128)(2,1)S(1)}, bf16[384,1024]{1,0:T(8,128)(2,1)S(1)}) custom-call(bf16[64,512]{1,0:T(8,128)(2,1)S(1)} %get-tuple-element.8.own_ref, bf16[64,512]{1,0:T(8,128)(2,1)S(1)} %collective-permute-done.1.other_ref, f32[1,1024]{1,0:T(1,128)S(1)} %bitcast.21, bf16[1024,1024]{1,0:T(8,128)(2,1)S(1)} %copy-done.1, ...), custom_call_target="tpu_custom_call" | custom-call | tf_op jit(solution)/shard_map/dispatch/pallas_call | solution.py:269
  16.8 29.6 %all_to_all.10 = bf16[16,24,1024]{2,1,0:T(8,128)(2,1)S(1)} all-to-all(bf16[16,24,1024]{2,1,0:T(8,128)(2,1)S(1)} %bitcast.15), channel_id=1, replica_groups=mesh['ep'=16,'tp'=2] {'ep'}, dimensions={0} | all-to-all | bytes 1572864 | tf_op jit(solution)/shard_map/all_to_all | solution.py:281
  46.4 0.0 collective-permute-start.2
  46.4 2.3 %collective-permute-done.2.other_ref = bf16[384,1024]{1,0:T(8,128)(2,1)S(1)} collective-permute-done((bf16[384,1024]{1,0:T(8,128)(2,1)S(1)}, bf16[384,1024]{1,0:T(8,128)(2,1)S(1)}, u32[]{:S(2)}, u32[]{:S(2)}) %collective-permute-start.2) | collective-permute-done | bytes 786464 | tf_op jit(solution)/shard_map/ppermute | solution.py:285
  48.7 0.0 copy-done.9
  48.7 10.0 %experts.1 = (bf16[384,1024]{1,0:T(8,128)(2,1)S(1)}, bf16[384,1024]{1,0:T(8,128)(2,1)S(1)}) custom-call(bf16[384,1024]{1,0:T(8,128)(2,1)S(1)} %bitcast.13, bf16[384,1024]{1,0:T(8,128)(2,1)S(1)} %collective-permute-done.2.other_ref, f32[1,2048]{1,0:T(1,128)S(1)} %bitcast.18, bf16[1,2048,1024]{2,1,0:T(8,128)(2,1)} %gate_ref.1, bf16[1,2048,1024]{2,1,0:T(8,128)(2,1)} %up_ref.1, ...), custom_call_target="tpu_custom_call" | custom-call | tf_op jit(solution)/shard_map/experts/pallas_call | solution.py:288
  58.7 0.0 copy-start.13
  58.7 0.2 collective-permute-start.3
  58.9 2.2 %collective-permute-done.3 = bf16[384,1024]{1,0:T(8,128)(2,1)S(1)} collective-permute-done((bf16[384,1024]{1,0:T(8,128)(2,1)S(1)}, bf16[384,1024]{1,0:T(8,128)(2,1)S(1)}, u32[]{:S(2)}, u32[]{:S(2)}) %collective-permute-start.3) | collective-permute-done | bytes 786464 | tf_op jit(solution)/shard_map/ppermute | solution.py:308
  61.1 0.3 add_convert_fusion
  61.4 24.7 %all_to_all.11 = bf16[16,24,1024]{2,1,0:T(8,128)(2,1)S(1)} all-to-all(bf16[16,24,1024]{2,1,0:T(8,128)(2,1)S(1)} %bitcast.25), channel_id=1, replica_groups=mesh['ep'=16,'tp'=2] {'ep'}, dimensions={0} | all-to-all | bytes 1572864 | tf_op jit(solution)/shard_map/all_to_all | solution.py:281
  86.1 0.0 copy-done.13
  86.1 1.2 %combine.1 = bf16[64,1024]{1,0:T(8,128)(2,1)} custom-call(s32[4,64]{1,0:T(4,128)S(1)} %bitcast.20, f32[4,64]{1,0:T(4,128)S(1)} %bitcast.23, bf16[64,1024]{1,0:T(8,128)(2,1)S(1)} %get-tuple-element.9.mid_ref, bf16[384,1024]{1,0:T(8,128)(2,1)S(1)} %bitcast.14), custom_call_target="tpu_custom_call" | custom-call | tf_op jit(solution)/shard_map/combine/pallas_call | solution.py:310
Async XLA Ops:
  0.6 1.8 %collective-permute-start = (bf16[64,1024]{1,0:T(8,128)(2,1)}, bf16[64,1024]{1,0:T(8,128)(2,1)S(1)}, u32[]{:S(2)}, u32[]{:S(2)}) collective-permute-start(bf16[64,1024]{1,0:T(8,128)(2,1)} %residual_ref.1), channel_id=1, source_target_pairs={{0,1},{1,0},{2,3},{3,2},{4,5},{5,4},{6,7},{7,6},{8,9},{9,8},{10,11... | collective-permute-start | bytes 393224 | tf_op jit(solution)/shard_map/ppermute | solution.py:245
  2.4 1.6 %copy-start = (bf16[2048,512]{1,0:T(8,128)(2,1)S(1)}, bf16[2048,512]{1,0:T(8,128)(2,1)}, u32[]{:S(2)}) copy-start(bf16[2048,512]{1,0:T(8,128)(2,1)} %proj_ref.2) | copy-start | bytes 6291460
  4.0 1.2 %copy-start.2 = (f32[2,64,2048]{2,1,0:T(8,128)S(1)}, f32[2,64,2048]{2,1,0:T(8,128)}, u32[]{:S(2)}) copy-start(f32[2,64,2048]{2,1,0:T(8,128)} %state_ref.1) | copy-start | bytes 3145732
  5.2 1.0 %copy-start.3 = (f32[2,32,64,16]{2,3,1,0:T(8,128)S(1)}, f32[2,32,64,16]{2,3,1,0:T(8,128)}, u32[]{:S(2)}) copy-start(f32[2,32,64,16]{2,3,1,0:T(8,128)} %param.27) | copy-start | bytes 786436
  6.2 1.0 %copy-start.4 = (f32[2,32,16,64]{3,2,1,0:T(8,128)S(1)}, f32[2,32,16,64]{3,2,1,0:T(8,128)}, u32[]{:S(2)}) copy-start(f32[2,32,16,64]{3,2,1,0:T(8,128)} %out_ref.1) | copy-start | bytes 786436
  7.3 0.9 %copy-start.5 = (bf16[64,1024]{1,0:T(8,128)(2,1)S(1)}, bf16[64,1024]{1,0:T(8,128)(2,1)}, u32[]{:S(2)}) copy-start(bf16[64,1024]{1,0:T(8,128)(2,1)} %residual_ref.1) | copy-start | bytes 393220
  8.2 0.7 copy-start.6
  8.9 0.7 copy-start.7
  9.6 0.7 copy-start.8
  10.3 0.7 copy-start.12
  11.0 0.7 copy-start.14
  11.7 4.2 %copy-start.1 = (bf16[1024,1024]{1,0:T(8,128)(2,1)S(1)}, bf16[1024,1024]{1,0:T(8,128)(2,1)}, u32[]{:S(2)}) copy-start(bf16[1024,1024]{1,0:T(8,128)(2,1)} %proj_ref.3) | copy-start | bytes 6291460
  11.7 4.2 %copy-start.10 = (s32[64,4]{0,1:T(4,128)S(1)}, s32[64,4]{0,1:T(4,128)}, u32[]{:S(2)}) copy-start(s32[64,4]{0,1:T(4,128)} %param.19) | copy-start | bytes 3076
  11.7 4.2 %copy-start.11 = (f32[1024]{0:T(1024)S(1)}, f32[1024]{0:T(1024)}, u32[]{:S(2)}) copy-start(f32[1024]{0:T(1024)} %param.30) | copy-start | bytes 12292
  14.6 34.1 %copy-start.9 = (f32[2048]{0:T(1024)S(1)}, f32[2048]{0:T(1024)}, u32[]{:S(2)}) copy-start(f32[2048]{0:T(1024)} %param.32) | copy-start | bytes 24580
  14.6 1.3 %collective-permute-start.1 = (bf16[64,512]{1,0:T(8,128)(2,1)S(1)}, bf16[64,512]{1,0:T(8,128)(2,1)S(1)}, u32[]{:S(2)}, u32[]{:S(2)}) collective-permute-start(bf16[64,512]{1,0:T(8,128)(2,1)S(1)} %get-tuple-element.8.own_ref), channel_id=1, source_target_pairs={{0,1},{1,0},{2,3},{3,2},{4,5},{5,4},{6,7},{7,6},{8,9},{9,8},{10,11... | collective-permute-start | bytes 196616 | tf_op jit(solution)/shard_map/ppermute | solution.py:267
  46.4 2.3 %collective-permute-start.2 = (bf16[384,1024]{1,0:T(8,128)(2,1)S(1)}, bf16[384,1024]{1,0:T(8,128)(2,1)S(1)}, u32[]{:S(2)}, u32[]{:S(2)}) collective-permute-start(bf16[384,1024]{1,0:T(8,128)(2,1)S(1)} %bitcast.12), channel_id=1, source_target_pairs={{0,1},{1,0},{2,3},{3,2},{4,5},{5,4},{6,7},{7,6},{8,9},{9,8},{10,11... | collective-permute-start | bytes 2359304 | tf_op jit(solution)/shard_map/ppermute | solution.py:285
  58.7 27.4 %copy-start.13 = (f32[64,4]{0,1:T(4,128)S(1)}, f32[64,4]{0,1:T(4,128)}, u32[]{:S(2)}) copy-start(f32[64,4]{0,1:T(4,128)} %param.20) | copy-start | bytes 3076
  58.7 2.4 %collective-permute-start.3 = (bf16[384,1024]{1,0:T(8,128)(2,1)S(1)}, bf16[384,1024]{1,0:T(8,128)(2,1)S(1)}, u32[]{:S(2)}, u32[]{:S(2)}) collective-permute-start(bf16[384,1024]{1,0:T(8,128)(2,1)S(1)} %get-tuple-element.12), channel_id=1, source_target_pairs={{0,1},{1,0},{2,3},{3,2},{4,5},{5,4},{6,7},{7,6},{8,9},{9,8},{10,11... | collective-permute-start | bytes 2359304 | tf_op jit(solution)/shard_map/ppermute | solution.py:308
